TPU v7x, 256 devices: a whole 4x4x8 slice. The times are simulated.
256 devices in a mesh: kv: 32 (over z, y), tp: 8 (over x, core).
Axes of the slice: x: 4, y: 4, z: 8, core: 2. Of those that a mesh axis runs over, the one named last changes fastest.
Arguments:
- tokens: bfloat16 [64, 4096], P(None, ('kv', 'tp')), may hold values from -8 to 8
- gate_weights: bfloat16 [2, 4096, 11264], P(None, None, ('kv', 'tp')), may hold values from -0.09375 to 0.09375
- up_weights: bfloat16 [2, 4096, 11264], P(None, None, ('kv', 'tp')), may hold values from -0.09375 to 0.09375
- down_weights: bfloat16 [2, 11264, 4096], P(None, ('kv', 'tp')), may hold values from -1 to 1
- norm_gain: bfloat16 [3, 4096], P(None, ('kv', 'tp')), may hold values from 0.25 to 4.5
- norm_bias: bfloat16 [3, 4096], P(None, ('kv', 'tp')), may hold values from -3 to 3
- query_weight: bfloat16 [4096, 4096], P('kv', 'tp'), may hold values from -0.09375 to 0.09375
- forget_weight: bfloat16 [4096, 4096], P('kv', 'tp'), may hold values from -0.09375 to 0.09375
- input_weight: bfloat16 [4096, 4096], P('kv', 'tp'), may hold values from -0.09375 to 0.09375
- outgate_weight: bfloat16 [4096, 4096], P('kv', 'tp'), may hold values from -0.09375 to 0.09375
- lower_bound: float32 [4096], P('tp'), may hold values from 0.05 to 0.9
- head_gain: float32 [4096], P('tp'), may hold values from 0.1 to 1.9
- out_weight: bfloat16 [4096, 4096], P('tp'), may hold values from -0.25 to 0.25
- state: float32 [64, 32, 128, 128], P('kv', 'tp'), may hold values from -3 to 3
Outputs:
- mixed: bfloat16 [64, 4096], P(None, ('kv', 'tp'))
- new_state: float32 [64, 32, 128, 128], P('kv', 'tp')
All inputs are finite; a program needn't handle non-finite values.
Results may differ from a plain program's by a relative error of at most 0.022.
Values may be sent and summed in bfloat16 or wider, within the bound.
No kernel may reach another device: no remote copies, remote signals or barrier semaphores. Data moves between devices by JAX's collectives and lax.ppermute only.
A program may use at most 64 MiB of HBM per device.

v0:
```python
import jax
import jax.numpy as jnp
from jax import lax
from jax.sharding import Mesh
from jax.sharding import PartitionSpec as P

HEAD = 128
KV_TP = ("kv_0", "kv_1", "tp_0", "tp_1")
KV = ("kv_0", "kv_1")
TP = ("tp_0", "tp_1")
residual_scale = 8.0**0.25
norm_eps = 1e-05
head_eps = 1e-06


def turned_gather(arrays, axis, dims):
    turned = [jnp.moveaxis(a, dim, 0) for a, dim in zip(arrays, dims)]
    both = jnp.concatenate([t.reshape(len(t), -1) for t in turned], axis=1)
    whole, at, gathered = (lax.all_gather(both, axis, axis=0, tiled=True), 0, [])
    for t, dim in zip(turned, dims):
        section = whole[:, at : at + t[0].size].reshape(-1, *t.shape[1:])
        gathered.append(jnp.moveaxis(section, 0, dim))
        at += t[0].size
    return tuple(gathered)


def rows_for(lines, count):
    spare = -lines.shape[0] % count
    if not spare:
        return lines
    return jnp.concatenate([lines, jnp.zeros((spare, *lines.shape[1:]), lines.dtype)])


def from_everyone(x, axis):
    copies = jnp.broadcast_to(x, (lax.axis_size(axis), *x.shape))
    return lax.all_to_all(copies, axis, split_axis=0, concat_axis=0, tiled=True)


def laid_out(blocks, dim):
    blocks = jnp.moveaxis(blocks, 0, dim)
    shape = blocks.shape
    return blocks.reshape(*shape[:dim], shape[dim] * shape[dim + 1], *shape[dim + 2 :])


def whole_of(x, axes, dim):
    far, near = axes
    leading = from_everyone(x, far)
    blocks = jnp.swapaxes(from_everyone(leading, near), 0, 1)
    return laid_out(blocks.reshape(-1, *x.shape), dim)


def in_blocks(x, dim, count):
    before, after = (x.shape[:dim], x.shape[dim + 1 :])
    return jnp.moveaxis(x.reshape(*before, count, -1, *after), dim, 0)


def sum_at_owner(x, axis, dim):
    blocks = in_blocks(x, dim, lax.axis_size(axis))
    arrived = lax.all_to_all(blocks, axis, split_axis=0, concat_axis=0, tiled=True)
    return arrived.sum(axis=0)


def sum_by_axis(x, axes, dim):
    far, near = axes
    blocks = in_blocks(x, dim, lax.axis_size(far))
    nearer = sum_at_owner(blocks, near, dim + 1)
    arrived = lax.all_to_all(nearer, far, split_axis=0, concat_axis=0, tiled=True)
    return arrived.sum(axis=0)


def nested_sum(x, axes):
    lines = x.reshape(-1)
    padded = rows_for(lines, lax.axis_size(axes[0]) * lax.axis_size(axes[1]))
    whole = whole_of(sum_by_axis(padded, axes, 0), axes, 0)
    return lax.slice_in_dim(whole, 0, len(lines)).reshape(x.shape)


def sum_at_owner_2(x, axis, dim):
    blocks = in_blocks(x, dim, lax.axis_size(axis))
    arrived = lax.all_to_all(blocks, axis, split_axis=0, concat_axis=0, tiled=True)
    return arrived.astype(jnp.float32).sum(axis=0)


def gathered_copies(x, axis, dim):
    blocks = from_everyone(x, axis)
    return laid_out(blocks, dim)


def whole_norm(stream, gain_row, bias_row):
    row_mean = jnp.mean(stream, axis=-1, keepdims=True)
    centred = stream - row_mean
    spread = jnp.mean(centred * centred, axis=-1, keepdims=True)
    return centred * lax.rsqrt(spread + norm_eps) * gain_row.astype(jnp.float32) + bias_row.astype(
        jnp.float32
    )


def ffn_partial(whole_rows, gate_w, up_w, down_w):
    gate_proj = jnp.dot(whole_rows, gate_w, preferred_element_type=jnp.float32)
    up_proj = jnp.dot(whole_rows, up_w, preferred_element_type=jnp.float32)
    hidden = (jax.nn.silu(gate_proj) * up_proj).astype(jnp.bfloat16)
    return jnp.dot(hidden, down_w, preferred_element_type=jnp.float32)


def local(
    tokens,
    gate_weights,
    up_weights,
    down_weights,
    norm_gain,
    norm_bias,
    query_weight,
    forget_weight,
    input_weight,
    outgate_weight,
    lower_bound,
    head_gain,
    out_weight,
    state,
):
    own_cols = tokens.shape[1]
    col_offset = lax.axis_index(KV_TP) * own_cols
    whole_tokens, whole_gain, whole_bias = turned_gather(
        (tokens, norm_gain, norm_bias), KV_TP, (1, 1, 1)
    )

    def finish(partial_value, residual_whole, index, want_whole):
        total = nested_sum(partial_value, (("kv_0", "kv_1"), ("tp_0", "tp_1")))
        stream = residual_scale * residual_whole + 0.5 * total
        normed = whole_norm(stream, whole_gain[index], whole_bias[index]).astype(jnp.bfloat16)
        if want_whole:
            return normed
        return lax.dynamic_slice_in_dim(normed, col_offset, own_cols, 1)

    partial_one = ffn_partial(whole_tokens, gate_weights[0], up_weights[0], down_weights[0])
    normed_one = finish(partial_one, whole_tokens.astype(jnp.float32), 0, True)
    seq_count = state.shape[0]
    head_count = state.shape[1]
    head_cols = query_weight.shape[1]
    weight_rows = query_weight.shape[0]
    seq_offset = lax.axis_index(KV) * seq_count
    block_rows = lax.dynamic_slice_in_dim(
        normed_one, lax.axis_index(KV) * weight_rows, weight_rows, 1
    )
    weights = (query_weight, forget_weight, input_weight, outgate_weight)
    projected = sum_at_owner_2(
        jnp.concatenate(
            [jnp.dot(block_rows, weight, preferred_element_type=jnp.float32) for weight in weights],
            axis=1,
        ).astype(jnp.bfloat16),
        KV,
        0,
    ).astype(jnp.bfloat16)
    query_pre = projected[:, :head_cols].astype(jnp.float32).reshape(seq_count, head_count, HEAD)
    forget_pre = (
        projected[:, head_cols : 2 * head_cols]
        .astype(jnp.float32)
        .reshape(seq_count, head_count, HEAD)
    )
    input_pre = (
        projected[:, 2 * head_cols : 3 * head_cols]
        .astype(jnp.float32)
        .reshape(seq_count, head_count, HEAD)
    )
    outgate_pre = projected[:, 3 * head_cols :].astype(jnp.float32)
    low_bound = lower_bound.reshape(head_count, HEAD)
    forget = low_bound + (1.0 - low_bound) * jax.nn.sigmoid(forget_pre)
    key_part = (1.0 - low_bound) * jax.nn.sigmoid(-forget_pre)
    updated = forget[..., None] * state + key_part[..., None] * input_pre[:, :, None, :]
    readout = jnp.einsum(
        "shd,shde->she", jax.nn.silu(query_pre), updated, precision=lax.Precision.HIGHEST
    )
    readout = readout * lax.rsqrt(jnp.mean(readout * readout, axis=-1, keepdims=True) + head_eps)
    gated_out = (
        readout.reshape(seq_count, head_cols) * head_gain * jax.nn.silu(outgate_pre)
    ).astype(jnp.bfloat16)
    mixer_part = jnp.dot(gated_out, out_weight, preferred_element_type=jnp.float32)
    head_sum = sum_at_owner_2(mixer_part.astype(jnp.bfloat16), TP, 1)
    piece_cols = head_sum.shape[1]
    own_normed = lax.dynamic_slice_in_dim(normed_one, seq_offset, seq_count, 0)
    own_normed = lax.dynamic_slice_in_dim(
        own_normed, lax.axis_index(TP) * piece_cols, piece_cols, 1
    )
    stream_own = (residual_scale * own_normed.astype(jnp.float32) + head_sum).astype(jnp.bfloat16)
    seq_rows = gathered_copies(stream_own, TP, 1)
    stream_two = gathered_copies(seq_rows, KV, 0)
    normed_two = whole_norm(stream_two.astype(jnp.float32), whole_gain[1], whole_bias[1]).astype(
        jnp.bfloat16
    )
    partial_two = ffn_partial(normed_two, gate_weights[1], up_weights[1], down_weights[1])
    mixed = finish(partial_two, normed_two.astype(jnp.float32), 2, False)
    return (mixed, updated)


def solution(mesh):
    finer = Mesh(mesh.devices.reshape(8, 4, 4, 2), ("kv_0", "kv_1", "tp_0", "tp_1"))
    in_specs = (
        P(None, KV_TP),
        P(None, None, KV_TP),
        P(None, None, KV_TP),
        P(None, KV_TP, None),
        P(None, KV_TP),
        P(None, KV_TP),
        P(KV, TP),
        P(KV, TP),
        P(KV, TP),
        P(KV, TP),
        P(TP),
        P(TP),
        P(TP, None),
        P(KV, TP, None, None),
    )
    out_specs = (P(None, KV_TP), P(KV, TP, None, None))
    return jax.shard_map(local, mesh=finer, in_specs=in_specs, out_specs=out_specs, check_vma=False)
```

profile of v0, /device:TPU:1, one launch (start us, length us, event | category | flops | bytes accessed | tf_op | source)
XLA Modules:
  0.0 302.1 jit_solution(11334063490553480618)
XLA Ops:
  3.0 67.7 %all_gather.3 = bf16[4096,70]{1,0:T(8,128)(2,1)S(1)} all-gather(bf16[16,70]{1,0:T(8,128)(2,1)S(1)} %pad_maximum_fusion.1), channel_id=1, replica_groups=mesh['kv_0'=8,'kv_1'=4,'tp_0'=4,'tp_1'=2] {'kv_0','kv_1','tp_0','tp_1'}, dimensions={0}, use_global_device_ids=true | all-gather | bytes 575680 | tf_op jit(solution)/shard_map/all_gather | solution.py:19
  70.8 4.6 %fusion.54 = (bf16[1,44,4096]{2,0,1:T(2,128)(2,1)}, bf16[1,44,4096]{2,0,1:T(2,128)(2,1)}) fusion(bf16[2,44,4096]{2,0,1:T(2,128)(2,1)} %param.17), kind=kLoop, calls=%fused_computation.115 | loop fusion | bytes 1441792 | tf_op jit(solution)/shard_map/slice | solution.py:190
  75.3 2.8 fusion.53
  83.7 18.4 %all_to_all.76 = f32[8,32,1024]{2,1,0:T(8,128)S(1)} all-to-all(f32[8,32,1024]{2,1,0:T(8,128)S(1)} %bitcast.90), channel_id=1, replica_groups=mesh['kv_0'=8,'kv_1'=4,'tp_0'=4,'tp_1'=2] {'tp_0','tp_1'}, dimensions={0} | all-to-all | bytes 2097152 | tf_op jit(solution)/shard_map/all_to_all | solution.py:59
  102.2 14.2 %all_to_all.77 = f32[32,1,1024]{2,1,0:T(1,128)S(1)} all-to-all(f32[32,1,1024]{2,1,0:T(1,128)S(1)} %all_to_all.49), channel_id=1, replica_groups=mesh['kv_0'=8,'kv_1'=4,'tp_0'=4,'tp_1'=2] {'kv_0','kv_1'}, dimensions={0} | all-to-all | bytes 262144 | tf_op jit(solution)/shard_map/all_to_all | solution.py:67
  117.3 3.9 %all-to-all-start.2 = ((f32[32,1,1024]{2,1,0:T(1,128)}), f32[32,1,1024]{2,1,0:T(1,128)S(1)}, u32[]{:S(2)}, u32[]{:S(2)}) async-start(f32[32,1,1024]{2,1,0:T(1,128)} %broadcast_in_dim.12), calls=%async_computation.2 | async-start | bytes 262144 | tf_op jit(solution)/shard_map/all_to_all | solution.py:36
  121.5 9.1 %all-to-all-done.2 = f32[32,1,1024]{2,1,0:T(1,128)S(1)} async-done(((f32[32,1,1024]{2,1,0:T(1,128)}), f32[32,1,1024]{2,1,0:T(1,128)S(1)}, u32[]{:S(2)}, u32[]{:S(2)}) %all-to-all-start.2) | async-done | bytes 131104 | tf_op jit(solution)/shard_map/all_to_all | solution.py:36
  131.7 7.1 %all-to-all-start.3 = ((f32[8,32,1024]{2,1,0:T(8,128)}), f32[8,32,1024]{2,1,0:T(8,128)S(1)}, u32[]{:S(2)}, u32[]{:S(2)}) async-start(f32[8,32,1024]{2,1,0:T(8,128)} %broadcast_in_dim.13), calls=%async_computation.3 | async-start | bytes 2097152 | tf_op jit(solution)/shard_map/all_to_all | solution.py:36
  139.5 3.4 %convert_reduce_fusion = (f32[4096]{0:T(1024)S(1)}, f32[4096]{0:T(1024)S(1)}, f32[4096]{0:T(1024)S(1)}, f32[4096]{0:T(1024)S(1)}, f32[4096]{0:T(1024)S(1)}, /*index=5*/f32[4096]{0:T(1024)S(1)}) fusion(bf16[3,4096]{0,1:T(8,128)(2,1)S(1)} %get-tuple-element.13, bf16[3,4096]{0,1:T(8,128)(2,1)S(1)} %get-tuple-element.12), kind=kLoop, calls=%fused_computation.1 | loop fusion | flops 24576 | bytes 147456 | tf_op jit(solution)/shard_map/add | solution.py:93
  142.8 11.0 %all-to-all-done.3 = f32[8,32,1024]{2,1,0:T(8,128)S(1)} async-done(((f32[8,32,1024]{2,1,0:T(8,128)}), f32[8,32,1024]{2,1,0:T(8,128)S(1)}, u32[]{:S(2)}, u32[]{:S(2)}) %all-to-all-start.3) | async-done | bytes 1048608 | tf_op jit(solution)/shard_map/all_to_all | solution.py:36
  157.7 3.9 %all-to-all-start.4 = ((bf16[32,2,2048]{2,1,0:T(2,128)(2,1)}), bf16[32,2,2048]{2,1,0:T(2,128)(2,1)S(1)}, u32[]{:S(2)}, u32[]{:S(2)}) async-start(bf16[32,2,2048]{2,1,0:T(2,128)(2,1)} %pad_maximum_fusion), calls=%async_computation.4 | async-start | bytes 524288 | tf_op jit(solution)/shard_map/all_to_all | solution.py:80
  161.6 11.4 %all-to-all-done.4 = bf16[32,2,2048]{2,1,0:T(2,128)(2,1)S(1)} async-done(((bf16[32,2,2048]{2,1,0:T(2,128)(2,1)}), bf16[32,2,2048]{2,1,0:T(2,128)(2,1)S(1)}, u32[]{:S(2)}, u32[]{:S(2)}) %all-to-all-start.4) | async-done | bytes 262176 | tf_op jit(solution)/shard_map/all_to_all | solution.py:80
  175.2 3.5 %convolution_convert_fusion = bf16[2,4096]{1,0:T(2,128)(2,1)} fusion(bf16[512,4096]{1,0:T(8,128)(2,1)} %param.26, f32[1,2,4,128]{3,2,1,0:T(4,128)S(1)} %multiply_bitcast_fusion.2, bf16[2,2048]{1,0:T(2,128)(2,1)S(1)} %reduce_sum.124, f32[512]{0:T(512)S(1)} %copy-done.12), kind=kOutput, calls=%fused_computation | convolution fusion | flops 8404992 | bytes 4218880 | tf_op jit(solution)/shard_map/dot_general | solution.py:177
  178.7 5.9 %all-to-all-start.5 = ((bf16[8,2,512]{2,1,0:T(2,128)(2,1)}), bf16[8,2,512]{2,1,0:T(2,128)(2,1)S(1)}, u32[]{:S(2)}, u32[]{:S(2)}) async-start(bf16[8,2,512]{2,1,0:T(2,128)(2,1)} %bitcast.17), calls=%async_computation.5 | async-start | bytes 32768 | tf_op jit(solution)/shard_map/all_to_all | solution.py:80
  184.6 4.7 %all-to-all-done.5 = bf16[8,2,512]{2,1,0:T(2,128)(2,1)S(1)} async-done(((bf16[8,2,512]{2,1,0:T(2,128)(2,1)}), bf16[8,2,512]{2,1,0:T(2,128)(2,1)S(1)}, u32[]{:S(2)}, u32[]{:S(2)}) %all-to-all-start.5) | async-done | bytes 16416 | tf_op jit(solution)/shard_map/all_to_all | solution.py:80
  189.4 7.7 %all_to_all.78 = bf16[8,2,512]{2,1,0:T(2,128)(2,1)S(1)} all-to-all(bf16[8,2,512]{2,1,0:T(2,128)(2,1)S(1)} %broadcast_in_dim.14), channel_id=1, replica_groups=mesh['kv_0'=8,'kv_1'=4,'tp_0'=4,'tp_1'=2] {'tp_0','tp_1'}, dimensions={0} | all-to-all | bytes 32768 | tf_op jit(solution)/shard_map/all_to_all | solution.py:36
  197.6 19.6 %all_to_all.79 = bf16[32,2,4096]{2,1,0:T(2,128)(2,1)S(1)} all-to-all(bf16[32,2,4096]{2,1,0:T(2,128)(2,1)S(1)} %broadcast_in_dim.15), channel_id=1, replica_groups=mesh['kv_0'=8,'kv_1'=4,'tp_0'=4,'tp_1'=2] {'kv_0','kv_1'}, dimensions={0} | all-to-all | bytes 1048576 | tf_op jit(solution)/shard_map/all_to_all | solution.py:36
  220.2 2.2 fusion.3
  223.4 19.7 %all_to_all.80 = f32[8,32,1024]{2,1,0:T(8,128)S(1)} all-to-all(f32[8,32,1024]{2,1,0:T(8,128)S(1)} %bitcast.91), channel_id=1, replica_groups=mesh['kv_0'=8,'kv_1'=4,'tp_0'=4,'tp_1'=2] {'tp_0','tp_1'}, dimensions={0} | all-to-all | bytes 2097152 | tf_op jit(solution)/shard_map/all_to_all | solution.py:59
  243.3 13.5 %all_to_all.81 = f32[32,1,1024]{2,1,0:T(1,128)S(1)} all-to-all(f32[32,1,1024]{2,1,0:T(1,128)S(1)} %all_to_all.59), channel_id=1, replica_groups=mesh['kv_0'=8,'kv_1'=4,'tp_0'=4,'tp_1'=2] {'kv_0','kv_1'}, dimensions={0} | all-to-all | bytes 262144 | tf_op jit(solution)/shard_map/all_to_all | solution.py:67
  257.6 3.9 %all-to-all-start.10 = ((f32[32,1,1024]{2,1,0:T(1,128)}), f32[32,1,1024]{2,1,0:T(1,128)S(1)}, u32[]{:S(2)}, u32[]{:S(2)}) async-start(f32[32,1,1024]{2,1,0:T(1,128)} %broadcast_in_dim.16), calls=%async_computation.10 | async-start | bytes 262144 | tf_op jit(solution)/shard_map/all_to_all | solution.py:36
  262.0 8.9 %all-to-all-done.10 = f32[32,1,1024]{2,1,0:T(1,128)S(1)} async-done(((f32[32,1,1024]{2,1,0:T(1,128)}), f32[32,1,1024]{2,1,0:T(1,128)S(1)}, u32[]{:S(2)}, u32[]{:S(2)}) %all-to-all-start.10) | async-done | bytes 131104 | tf_op jit(solution)/shard_map/all_to_all | solution.py:36
  272.1 7.1 %all-to-all-start.11 = ((f32[8,32,1024]{2,1,0:T(8,128)}), f32[8,32,1024]{2,1,0:T(8,128)S(1)}, u32[]{:S(2)}, u32[]{:S(2)}) async-start(f32[8,32,1024]{2,1,0:T(8,128)} %broadcast_in_dim.17), calls=%async_computation.11 | async-start | bytes 2097152 | tf_op jit(solution)/shard_map/all_to_all | solution.py:36
  280.4 13.8 %all-to-all-done.11 = f32[8,32,1024]{2,1,0:T(8,128)S(1)} async-done(((f32[8,32,1024]{2,1,0:T(8,128)}), f32[8,32,1024]{2,1,0:T(8,128)S(1)}, u32[]{:S(2)}, u32[]{:S(2)}) %all-to-all-start.11) | async-done | bytes 1048608 | tf_op jit(solution)/shard_map/all_to_all | solution.py:36
  (113 shorter events, 33.2 us)
Async XLA Ops:
  0.6 155.3 %copy-start = (bf16[128,512]{1,0:T(8,128)(2,1)S(1)}, bf16[128,512]{1,0:T(8,128)(2,1)}, u32[]{:S(2)}) copy-start(bf16[128,512]{1,0:T(8,128)(2,1)} %param.23) | copy-start | bytes 393220
  0.6 74.7 %copy-start.1 = (bf16[2,4096,44]{1,0,2:T(2,128)(2,1)S(1)}, bf16[2,4096,44]{1,0,2:T(2,128)(2,1)}, u32[]{:S(2)}) copy-start(bf16[2,4096,44]{1,0,2:T(2,128)(2,1)} %param.16) | copy-start | bytes 2162692
  75.3 2.8 copy-start.2
  78.1 2.4 copy-start.6
  117.3 13.3 %all-to-all-start.2 = ((f32[32,1,1024]{2,1,0:T(1,128)}), f32[32,1,1024]{2,1,0:T(1,128)S(1)}, u32[]{:S(2)}, u32[]{:S(2)}) async-start(f32[32,1,1024]{2,1,0:T(1,128)} %broadcast_in_dim.12), calls=%async_computation.2 | async-start | bytes 262144 | tf_op jit(solution)/shard_map/all_to_all | solution.py:36
  131.7 22.1 %all-to-all-start.3 = ((f32[8,32,1024]{2,1,0:T(8,128)}), f32[8,32,1024]{2,1,0:T(8,128)S(1)}, u32[]{:S(2)}, u32[]{:S(2)}) async-start(f32[8,32,1024]{2,1,0:T(8,128)} %broadcast_in_dim.13), calls=%async_computation.3 | async-start | bytes 2097152 | tf_op jit(solution)/shard_map/all_to_all | solution.py:36
  155.3 0.9 copy-start.8
  155.3 1.1 copy-start.9
  155.3 1.3 copy-start.10
  155.6 6.0 %copy-start.11 = (f32[512]{0:T(512)S(1)}, f32[512]{0:T(512)}, u32[]{:S(2)}) copy-start(f32[512]{0:T(512)} %param.24) | copy-start | bytes 6148
  155.6 17.7 %copy-start.7 = (f32[2,4,128,128]{3,2,1,0:T(8,128)S(1)}, f32[2,4,128,128]{3,2,1,0:T(8,128)}, u32[]{:S(2)}) copy-start(f32[2,4,128,128]{3,2,1,0:T(8,128)} %param.27) | copy-start | bytes 1572868
  156.1 19.1 %copy-start.12 = (f32[512]{0:T(512)S(1)}, f32[512]{0:T(512)}, u32[]{:S(2)}) copy-start(f32[512]{0:T(512)} %param.25) | copy-start | bytes 6148
  157.7 15.3 %all-to-all-start.4 = ((bf16[32,2,2048]{2,1,0:T(2,128)(2,1)}), bf16[32,2,2048]{2,1,0:T(2,128)(2,1)S(1)}, u32[]{:S(2)}, u32[]{:S(2)}) async-start(bf16[32,2,2048]{2,1,0:T(2,128)(2,1)} %pad_maximum_fusion), calls=%async_computation.4 | async-start | bytes 524288 | tf_op jit(solution)/shard_map/all_to_all | solution.py:80
  173.7 0.8 copy-start.3
  178.7 10.6 %all-to-all-start.5 = ((bf16[8,2,512]{2,1,0:T(2,128)(2,1)}), bf16[8,2,512]{2,1,0:T(2,128)(2,1)S(1)}, u32[]{:S(2)}, u32[]{:S(2)}) async-start(bf16[8,2,512]{2,1,0:T(2,128)(2,1)} %bitcast.17), calls=%async_computation.5 | async-start | bytes 32768 | tf_op jit(solution)/shard_map/all_to_all | solution.py:80
  197.6 22.1 %copy-start.5 = (bf16[1,4096,44]{1,0,2:T(2,128)(2,1)S(1)}, bf16[1,4096,44]{1,0,2:T(2,128)(2,1)}, u32[]{:S(2)}) copy-start(bf16[1,4096,44]{1,0,2:T(2,128)(2,1)} %get-tuple-element.14) | copy-start | bytes 1081348
  217.2 3.1 %copy-start.4 = (bf16[1,44,4096]{2,0,1:T(2,128)(2,1)S(1)}, bf16[1,44,4096]{2,0,1:T(2,128)(2,1)}, u32[]{:S(2)}) copy-start(bf16[1,44,4096]{2,0,1:T(2,128)(2,1)} %get-tuple-element.18) | copy-start | bytes 1081348
  257.6 13.3 %all-to-all-start.10 = ((f32[32,1,1024]{2,1,0:T(1,128)}), f32[32,1,1024]{2,1,0:T(1,128)S(1)}, u32[]{:S(2)}, u32[]{:S(2)}) async-start(f32[32,1,1024]{2,1,0:T(1,128)} %broadcast_in_dim.16), calls=%async_computation.10 | async-start | bytes 262144 | tf_op jit(solution)/shard_map/all_to_all | solution.py:36
  272.1 22.1 %all-to-all-start.11 = ((f32[8,32,1024]{2,1,0:T(8,128)}), f32[8,32,1024]{2,1,0:T(8,128)S(1)}, u32[]{:S(2)}, u32[]{:S(2)}) async-start(f32[8,32,1024]{2,1,0:T(8,128)} %broadcast_in_dim.17), calls=%async_computation.11 | async-start | bytes 2097152 | tf_op jit(solution)/shard_map/all_to_all | solution.py:36
where the time goes:
time: 303 us; the launch traced here: 302 us
  blocking collectives  161 us (53%)
  waiting for transfers between devices  58.8 us (19%)
  starting transfers between devices  31.7 us (10%)
  local copies, waits for them, and re-layouts  24.7 us (8%)
  other arithmetic  14.9 us (5%)
  matrix products  10 us (3%)
    all_gather x1, blocking collectives, turned_gather(): lax.all_gather(both, axis, axis=0, tiled=True)  67.7 us
    all_to_all x4, waiting for transfers between devices, from_everyone(): return lax.all_to_all(copies, axis, split_axis=0, concat_axis=0, tiled=True)  42.7 us
    all_to_all x2, blocking collectives, sum_at_owner(): lax.all_to_all(blocks, axis, split_axis=0, concat_axis=0, tiled=True)  38.1 us
    all_to_all x2, blocking collectives, sum_by_axis(): lax.all_to_all(nearer, far, split_axis=0, concat_axis=0, tiled=True)  27.8 us
    all_to_all x2, blocking collectives, from_everyone(): return lax.all_to_all(copies, axis, split_axis=0, concat_axis=0, tiled=True)  27.3 us
    all_to_all x4, starting transfers between devices, from_everyone(): return lax.all_to_all(copies, axis, split_axis=0, concat_axis=0, tiled=True)  22 us
    all_to_all x2, waiting for transfers between devices, sum_at_owner_2(): lax.all_to_all(blocks, axis, split_axis=0, concat_axis=0, tiled=True)  16.1 us
    all_to_all x2, starting transfers between devices, sum_at_owner_2(): lax.all_to_all(blocks, axis, split_axis=0, concat_axis=0, tiled=True)  9.75 us
  transfers between devices with their start and end apart: 6, of which 6 were waited for; matrix products, arithmetic and copies ran while one was open for 2% of the time, Pallas kernels for 0%

commit v1 on v0

--- a/solution.py
+++ b/solution.py
@@ -16,7 +16,13 @@
 def turned_gather(arrays, axis, dims):
     turned = [jnp.moveaxis(a, dim, 0) for a, dim in zip(arrays, dims)]
     both = jnp.concatenate([t.reshape(len(t), -1) for t in turned], axis=1)
-    whole, at, gathered = (lax.all_gather(both, axis, axis=0, tiled=True), 0, [])
+    whole, at, gathered = (
+        jnp.concatenate(
+            lax.all_to_all(jnp.stack([both] * lax.axis_size(axis)), axis, 0, 0), axis=0
+        ),
+        0,
+        [],
+    )
     for t, dim in zip(turned, dims):
         section = whole[:, at : at + t[0].size].reshape(-1, *t.shape[1:])
         gathered.append(jnp.moveaxis(section, 0, dim))

time: 303 us -> 273 us (0.901)
  blocking collectives: 161 us -> 93 us
  waiting for transfers between devices: 58.8 us -> 81.2 us
  starting transfers between devices: 31.7 us -> 47.3 us
    all_gather x1 -> x0, blocking collectives: 67.7 us -> none  [turned_gather(): lax.all_gather(both, axis, axis=0, tiled=True)]
    all_to_all x0 -> x1, waiting for transfers between devices: none -> 22.4 us  [turned_gather(): lax.all_to_all(jnp.stack([both] * lax.axis_size(axis)), axis, 0, 0)]
    all_to_all x0 -> x1, starting transfers between devices: none -> 15.6 us  [turned_gather(): lax.all_to_all(jnp.stack([both] * lax.axis_size(axis)), axis, 0, 0)]
  transfers between devices with their start and end apart: 6 -> 7, of which waited for: 6 -> 7; matrix products, arithmetic and copies ran while one was open for 2% -> 5% of each run, Pallas kernels for 0% -> 0%
where the time goes in v1:
time: 273 us; the launch traced here: 272 us
  blocking collectives  93 us (34%)
  waiting for transfers between devices  81.2 us (30%)
  starting transfers between devices  47.3 us (17%)
  local copies, waits for them, and re-layouts  24.7 us (9%)
  other arithmetic  14.8 us (5%)
  matrix products  10.2 us (4%)
    all_to_all x4, waiting for transfers between devices, from_everyone(): return lax.all_to_all(copies, axis, split_axis=0, concat_axis=0, tiled=True)  42.7 us
    all_to_all x2, blocking collectives, sum_at_owner(): lax.all_to_all(blocks, axis, split_axis=0, concat_axis=0, tiled=True)  39.7 us
    all_to_all x2, blocking collectives, from_everyone(): return lax.all_to_all(copies, axis, split_axis=0, concat_axis=0, tiled=True)  27.3 us
    all_to_all x2, blocking collectives, sum_by_axis(): lax.all_to_all(nearer, far, split_axis=0, concat_axis=0, tiled=True)  26 us
    all_to_all x1, waiting for transfers between devices, turned_gather(): lax.all_to_all(jnp.stack([both] * lax.axis_size(axis)), axis, 0, 0)  22.4 us
    all_to_all x4, starting transfers between devices, from_everyone(): return lax.all_to_all(copies, axis, split_axis=0, concat_axis=0, tiled=True)  22 us
    all_to_all x2, waiting for transfers between devices, sum_at_owner_2(): lax.all_to_all(blocks, axis, split_axis=0, concat_axis=0, tiled=True)  16.1 us
    all_to_all x1, starting transfers between devices, turned_gather(): lax.all_to_all(jnp.stack([both] * lax.axis_size(axis)), axis, 0, 0)  15.6 us
  transfers between devices with their start and end apart: 7, of which 7 were waited for; matrix products, arithmetic and copies ran while one was open for 5% of the time, Pallas kernels for 0%

profile of v1, /device:TPU:1, one launch (start us, length us, event | category | flops | bytes accessed | tf_op | source)
XLA Modules:
  0.0 272.5 jit_solution(3084040128954077170)
XLA Ops:
  4.2 15.6 %all-to-all-start = ((bf16[256,16,70]{2,1,0:T(8,128)(2,1)}), bf16[256,16,70]{2,1,0:T(8,128)(2,1)S(1)}, u32[]{:S(2)}, u32[]{:S(2)}) async-start(bf16[256,16,70]{2,1,0:T(8,128)(2,1)} %stack.2), calls=%async_computation | async-start | bytes 2097152 | tf_op jit(solution)/shard_map/all_to_all | solution.py:21
  19.8 2.8 %fusion.54 = (bf16[1,44,4096]{2,0,1:T(2,128)(2,1)}, bf16[1,44,4096]{2,0,1:T(2,128)(2,1)}) fusion(bf16[2,44,4096]{2,0,1:T(2,128)(2,1)S(1)} %copy-done.1), kind=kLoop, calls=%fused_computation.115 | loop fusion | bytes 1441792 | tf_op jit(solution)/shard_map/slice | solution.py:196
  22.6 2.8 %fusion.53 = (bf16[1,4096,44]{1,0,2:T(2,128)(2,1)}, bf16[1,4096,44]{1,0,2:T(2,128)(2,1)}) fusion(bf16[2,4096,44]{1,0,2:T(2,128)(2,1)S(1)} %copy-done.2), kind=kLoop, calls=%fused_computation.114 | loop fusion | bytes 1441792 | tf_op jit(solution)/shard_map/slice | solution.py:196
  28.0 22.4 %all-to-all-done = bf16[256,16,70]{2,1,0:T(8,128)(2,1)S(1)} async-done(((bf16[256,16,70]{2,1,0:T(8,128)(2,1)}), bf16[256,16,70]{2,1,0:T(8,128)(2,1)S(1)}, u32[]{:S(2)}, u32[]{:S(2)}) %all-to-all-start) | async-done | bytes 573472 | tf_op jit(solution)/shard_map/all_to_all | solution.py:21
  54.2 19.9 %all_to_all.81 = f32[8,32,1024]{2,1,0:T(8,128)S(1)} all-to-all(f32[8,32,1024]{2,1,0:T(8,128)S(1)} %bitcast.94), channel_id=1, replica_groups=mesh['kv_0'=8,'kv_1'=4,'tp_0'=4,'tp_1'=2] {'tp_0','tp_1'}, dimensions={0} | all-to-all | bytes 2097152 | tf_op jit(solution)/shard_map/all_to_all | solution.py:65
  74.4 12.5 %all_to_all.82 = f32[32,1,1024]{2,1,0:T(1,128)S(1)} all-to-all(f32[32,1,1024]{2,1,0:T(1,128)S(1)} %all_to_all.53), channel_id=1, replica_groups=mesh['kv_0'=8,'kv_1'=4,'tp_0'=4,'tp_1'=2] {'kv_0','kv_1'}, dimensions={0} | all-to-all | bytes 262144 | tf_op jit(solution)/shard_map/all_to_all | solution.py:73
  87.7 3.9 %all-to-all-start.3 = ((f32[32,1,1024]{2,1,0:T(1,128)}), f32[32,1,1024]{2,1,0:T(1,128)S(1)}, u32[]{:S(2)}, u32[]{:S(2)}) async-start(f32[32,1,1024]{2,1,0:T(1,128)} %broadcast_in_dim.12), calls=%async_computation.3 | async-start | bytes 262144 | tf_op jit(solution)/shard_map/all_to_all | solution.py:42
  91.9 9.1 %all-to-all-done.3 = f32[32,1,1024]{2,1,0:T(1,128)S(1)} async-done(((f32[32,1,1024]{2,1,0:T(1,128)}), f32[32,1,1024]{2,1,0:T(1,128)S(1)}, u32[]{:S(2)}, u32[]{:S(2)}) %all-to-all-start.3) | async-done | bytes 131104 | tf_op jit(solution)/shard_map/all_to_all | solution.py:42
  102.1 7.1 %all-to-all-start.4 = ((f32[8,32,1024]{2,1,0:T(8,128)}), f32[8,32,1024]{2,1,0:T(8,128)S(1)}, u32[]{:S(2)}, u32[]{:S(2)}) async-start(f32[8,32,1024]{2,1,0:T(8,128)} %broadcast_in_dim.13), calls=%async_computation.4 | async-start | bytes 2097152 | tf_op jit(solution)/shard_map/all_to_all | solution.py:42
  109.8 3.4 %convert_reduce_fusion = (f32[4096]{0:T(1024)S(1)}, f32[4096]{0:T(1024)S(1)}, f32[4096]{0:T(1024)S(1)}, f32[4096]{0:T(1024)S(1)}, f32[4096]{0:T(1024)S(1)}, /*index=5*/f32[4096]{0:T(1024)S(1)}) fusion(bf16[3,4096]{0,1:T(8,128)(2,1)S(1)} %get-tuple-element.17, bf16[3,4096]{0,1:T(8,128)(2,1)S(1)} %get-tuple-element.16), kind=kLoop, calls=%fused_computation.1 | loop fusion | flops 24576 | bytes 147456 | tf_op jit(solution)/shard_map/add | solution.py:99
  113.2 11.0 %all-to-all-done.4 = f32[8,32,1024]{2,1,0:T(8,128)S(1)} async-done(((f32[8,32,1024]{2,1,0:T(8,128)}), f32[8,32,1024]{2,1,0:T(8,128)S(1)}, u32[]{:S(2)}, u32[]{:S(2)}) %all-to-all-start.4) | async-done | bytes 1048608 | tf_op jit(solution)/shard_map/all_to_all | solution.py:42
  128.1 3.9 %all-to-all-start.5 = ((bf16[32,2,2048]{2,1,0:T(2,128)(2,1)}), bf16[32,2,2048]{2,1,0:T(2,128)(2,1)S(1)}, u32[]{:S(2)}, u32[]{:S(2)}) async-start(bf16[32,2,2048]{2,1,0:T(2,128)(2,1)} %pad_maximum_fusion), calls=%async_computation.5 | async-start | bytes 524288 | tf_op jit(solution)/shard_map/all_to_all | solution.py:86
  132.0 11.4 %all-to-all-done.5 = bf16[32,2,2048]{2,1,0:T(2,128)(2,1)S(1)} async-done(((bf16[32,2,2048]{2,1,0:T(2,128)(2,1)}), bf16[32,2,2048]{2,1,0:T(2,128)(2,1)S(1)}, u32[]{:S(2)}, u32[]{:S(2)}) %all-to-all-start.5) | async-done | bytes 262176 | tf_op jit(solution)/shard_map/all_to_all | solution.py:86
  145.6 3.5 %convolution_convert_fusion = bf16[2,4096]{1,0:T(2,128)(2,1)} fusion(bf16[512,4096]{1,0:T(8,128)(2,1)} %param.26, f32[1,2,4,128]{3,2,1,0:T(4,128)S(1)} %multiply_bitcast_fusion.2, bf16[2,2048]{1,0:T(2,128)(2,1)S(1)} %reduce_sum.124, f32[512]{0:T(512)S(1)} %copy-done.12), kind=kOutput, calls=%fused_computation | convolution fusion | flops 8404992 | bytes 4218880 | tf_op jit(solution)/shard_map/dot_general | solution.py:183
  149.0 5.9 %all-to-all-start.6 = ((bf16[8,2,512]{2,1,0:T(2,128)(2,1)}), bf16[8,2,512]{2,1,0:T(2,128)(2,1)S(1)}, u32[]{:S(2)}, u32[]{:S(2)}) async-start(bf16[8,2,512]{2,1,0:T(2,128)(2,1)} %bitcast.18), calls=%async_computation.6 | async-start | bytes 32768 | tf_op jit(solution)/shard_map/all_to_all | solution.py:86
  154.9 4.7 %all-to-all-done.6 = bf16[8,2,512]{2,1,0:T(2,128)(2,1)S(1)} async-done(((bf16[8,2,512]{2,1,0:T(2,128)(2,1)}), bf16[8,2,512]{2,1,0:T(2,128)(2,1)S(1)}, u32[]{:S(2)}, u32[]{:S(2)}) %all-to-all-start.6) | async-done | bytes 16416 | tf_op jit(solution)/shard_map/all_to_all | solution.py:86
  159.7 7.7 %all_to_all.83 = bf16[8,2,512]{2,1,0:T(2,128)(2,1)S(1)} all-to-all(bf16[8,2,512]{2,1,0:T(2,128)(2,1)S(1)} %broadcast_in_dim.14), channel_id=1, replica_groups=mesh['kv_0'=8,'kv_1'=4,'tp_0'=4,'tp_1'=2] {'tp_0','tp_1'}, dimensions={0} | all-to-all | bytes 32768 | tf_op jit(solution)/shard_map/all_to_all | solution.py:42
  167.9 19.6 %all_to_all.84 = bf16[32,2,4096]{2,1,0:T(2,128)(2,1)S(1)} all-to-all(bf16[32,2,4096]{2,1,0:T(2,128)(2,1)S(1)} %broadcast_in_dim.15), channel_id=1, replica_groups=mesh['kv_0'=8,'kv_1'=4,'tp_0'=4,'tp_1'=2] {'kv_0','kv_1'}, dimensions={0} | all-to-all | bytes 1048576 | tf_op jit(solution)/shard_map/all_to_all | solution.py:42
  193.7 19.7 %all_to_all.85 = f32[8,32,1024]{2,1,0:T(8,128)S(1)} all-to-all(f32[8,32,1024]{2,1,0:T(8,128)S(1)} %bitcast.95), channel_id=1, replica_groups=mesh['kv_0'=8,'kv_1'=4,'tp_0'=4,'tp_1'=2] {'tp_0','tp_1'}, dimensions={0} | all-to-all | bytes 2097152 | tf_op jit(solution)/shard_map/all_to_all | solution.py:65
  213.6 13.5 %all_to_all.86 = f32[32,1,1024]{2,1,0:T(1,128)S(1)} all-to-all(f32[32,1,1024]{2,1,0:T(1,128)S(1)} %all_to_all.63), channel_id=1, replica_groups=mesh['kv_0'=8,'kv_1'=4,'tp_0'=4,'tp_1'=2] {'kv_0','kv_1'}, dimensions={0} | all-to-all | bytes 262144 | tf_op jit(solution)/shard_map/all_to_all | solution.py:73
  228.0 3.9 %all-to-all-start.11 = ((f32[32,1,1024]{2,1,0:T(1,128)}), f32[32,1,1024]{2,1,0:T(1,128)S(1)}, u32[]{:S(2)}, u32[]{:S(2)}) async-start(f32[32,1,1024]{2,1,0:T(1,128)} %broadcast_in_dim.16), calls=%async_computation.11 | async-start | bytes 262144 | tf_op jit(solution)/shard_map/all_to_all | solution.py:42
  232.4 8.9 %all-to-all-done.11 = f32[32,1,1024]{2,1,0:T(1,128)S(1)} async-done(((f32[32,1,1024]{2,1,0:T(1,128)}), f32[32,1,1024]{2,1,0:T(1,128)S(1)}, u32[]{:S(2)}, u32[]{:S(2)}) %all-to-all-start.11) | async-done | bytes 131104 | tf_op jit(solution)/shard_map/all_to_all | solution.py:42
  242.4 7.1 %all-to-all-start.12 = ((f32[8,32,1024]{2,1,0:T(8,128)}), f32[8,32,1024]{2,1,0:T(8,128)S(1)}, u32[]{:S(2)}, u32[]{:S(2)}) async-start(f32[8,32,1024]{2,1,0:T(8,128)} %broadcast_in_dim.17), calls=%async_computation.12 | async-start | bytes 2097152 | tf_op jit(solution)/shard_map/all_to_all | solution.py:42
  250.8 13.8 %all-to-all-done.12 = f32[8,32,1024]{2,1,0:T(8,128)S(1)} async-done(((f32[8,32,1024]{2,1,0:T(8,128)}), f32[8,32,1024]{2,1,0:T(8,128)S(1)}, u32[]{:S(2)}, u32[]{:S(2)}) %all-to-all-start.12) | async-done | bytes 1048608 | tf_op jit(solution)/shard_map/all_to_all | solution.py:42
  (115 shorter events, 37.4 us)
Async XLA Ops:
  0.6 125.7 %copy-start = (bf16[128,512]{1,0:T(8,128)(2,1)S(1)}, bf16[128,512]{1,0:T(8,128)(2,1)}, u32[]{:S(2)}) copy-start(bf16[128,512]{1,0:T(8,128)(2,1)} %param.23) | copy-start | bytes 393220
  0.6 19.2 %copy-start.1 = (bf16[2,44,4096]{2,0,1:T(2,128)(2,1)S(1)}, bf16[2,44,4096]{2,0,1:T(2,128)(2,1)}, u32[]{:S(2)}) copy-start(bf16[2,44,4096]{2,0,1:T(2,128)(2,1)} %param.17) | copy-start | bytes 2162692
  4.2 18.5 %copy-start.2 = (bf16[2,4096,44]{1,0,2:T(2,128)(2,1)S(1)}, bf16[2,4096,44]{1,0,2:T(2,128)(2,1)}, u32[]{:S(2)}) copy-start(bf16[2,4096,44]{1,0,2:T(2,128)(2,1)} %param.16) | copy-start | bytes 2162692
  4.2 46.2 %all-to-all-start = ((bf16[256,16,70]{2,1,0:T(8,128)(2,1)}), bf16[256,16,70]{2,1,0:T(8,128)(2,1)S(1)}, u32[]{:S(2)}, u32[]{:S(2)}) async-start(bf16[256,16,70]{2,1,0:T(8,128)(2,1)} %stack.2), calls=%async_computation | async-start | bytes 2097152 | tf_op jit(solution)/shard_map/all_to_all | solution.py:21
  22.6 2.8 %copy-start.3 = (bf16[2,4096,44]{1,0,2:T(2,128)(2,1)S(1)}, bf16[2,4096,44]{1,0,2:T(2,128)(2,1)}, u32[]{:S(2)}) copy-start(bf16[2,4096,44]{1,0,2:T(2,128)(2,1)} %param.15) | copy-start | bytes 2162692
  87.7 13.3 %all-to-all-start.3 = ((f32[32,1,1024]{2,1,0:T(1,128)}), f32[32,1,1024]{2,1,0:T(1,128)S(1)}, u32[]{:S(2)}, u32[]{:S(2)}) async-start(f32[32,1,1024]{2,1,0:T(1,128)} %broadcast_in_dim.12), calls=%async_computation.3 | async-start | bytes 262144 | tf_op jit(solution)/shard_map/all_to_all | solution.py:42
  102.1 22.1 %all-to-all-start.4 = ((f32[8,32,1024]{2,1,0:T(8,128)}), f32[8,32,1024]{2,1,0:T(8,128)S(1)}, u32[]{:S(2)}, u32[]{:S(2)}) async-start(f32[8,32,1024]{2,1,0:T(8,128)} %broadcast_in_dim.13), calls=%async_computation.4 | async-start | bytes 2097152 | tf_op jit(solution)/shard_map/all_to_all | solution.py:42
  125.6 0.9 copy-start.8
  125.6 1.1 copy-start.9
  125.7 1.3 copy-start.10
  126.0 6.0 %copy-start.11 = (f32[512]{0:T(512)S(1)}, f32[512]{0:T(512)}, u32[]{:S(2)}) copy-start(f32[512]{0:T(512)} %param.24) | copy-start | bytes 6148
  126.0 17.7 %copy-start.7 = (f32[2,4,128,128]{3,2,1,0:T(8,128)S(1)}, f32[2,4,128,128]{3,2,1,0:T(8,128)}, u32[]{:S(2)}) copy-start(f32[2,4,128,128]{3,2,1,0:T(8,128)} %param.27) | copy-start | bytes 1572868
  126.5 19.1 %copy-start.12 = (f32[512]{0:T(512)S(1)}, f32[512]{0:T(512)}, u32[]{:S(2)}) copy-start(f32[512]{0:T(512)} %param.25) | copy-start | bytes 6148
  128.1 15.3 %all-to-all-start.5 = ((bf16[32,2,2048]{2,1,0:T(2,128)(2,1)}), bf16[32,2,2048]{2,1,0:T(2,128)(2,1)S(1)}, u32[]{:S(2)}, u32[]{:S(2)}) async-start(bf16[32,2,2048]{2,1,0:T(2,128)(2,1)} %pad_maximum_fusion), calls=%async_computation.5 | async-start | bytes 524288 | tf_op jit(solution)/shard_map/all_to_all | solution.py:86
  144.1 0.8 copy-start.4
  149.0 10.6 %all-to-all-start.6 = ((bf16[8,2,512]{2,1,0:T(2,128)(2,1)}), bf16[8,2,512]{2,1,0:T(2,128)(2,1)S(1)}, u32[]{:S(2)}, u32[]{:S(2)}) async-start(bf16[8,2,512]{2,1,0:T(2,128)(2,1)} %bitcast.18), calls=%async_computation.6 | async-start | bytes 32768 | tf_op jit(solution)/shard_map/all_to_all | solution.py:86
  167.9 22.1 %copy-start.6 = (bf16[1,4096,44]{1,0,2:T(2,128)(2,1)S(1)}, bf16[1,4096,44]{1,0,2:T(2,128)(2,1)}, u32[]{:S(2)}) copy-start(bf16[1,4096,44]{1,0,2:T(2,128)(2,1)} %get-tuple-element.18) | copy-start | bytes 1081348
  187.5 3.1 %copy-start.5 = (bf16[1,44,4096]{2,0,1:T(2,128)(2,1)S(1)}, bf16[1,44,4096]{2,0,1:T(2,128)(2,1)}, u32[]{:S(2)}) copy-start(bf16[1,44,4096]{2,0,1:T(2,128)(2,1)} %get-tuple-element.22) | copy-start | bytes 1081348
  228.0 13.3 %all-to-all-start.11 = ((f32[32,1,1024]{2,1,0:T(1,128)}), f32[32,1,1024]{2,1,0:T(1,128)S(1)}, u32[]{:S(2)}, u32[]{:S(2)}) async-start(f32[32,1,1024]{2,1,0:T(1,128)} %broadcast_in_dim.16), calls=%async_computation.11 | async-start | bytes 262144 | tf_op jit(solution)/shard_map/all_to_all | solution.py:42
  242.4 22.1 %all-to-all-start.12 = ((f32[8,32,1024]{2,1,0:T(8,128)}), f32[8,32,1024]{2,1,0:T(8,128)S(1)}, u32[]{:S(2)}, u32[]{:S(2)}) async-start(f32[8,32,1024]{2,1,0:T(8,128)} %broadcast_in_dim.17), calls=%async_computation.12 | async-start | bytes 2097152 | tf_op jit(solution)/shard_map/all_to_all | solution.py:42
